TPU v7x, 512 devices: a whole 4x8x8 slice. The times are simulated.
512 devices in a mesh: sp: 32 (over z, x), tp: 16 (over y, core).
Axes of the slice: x: 4, y: 8, z: 8, core: 2. Of those that a mesh axis runs over, the one named last changes fastest.
Arguments:
- queries: bfloat16 [8192, 1024], P('sp', 'tp'), may hold values from -6 to 6
- keys: bfloat16 [8192, 256], P('sp'), may hold values from -6 to 6
- values: bfloat16 [8192, 256], P('sp'), may hold values from -6 to 6
- sink: float32 [16], P('tp'), may hold values from 3 to 6
- w_out: bfloat16 [1024, 2048], P('tp'), may hold values from -0.1875 to 0.1875
- stream: bfloat16 [8192, 2048], P(('sp', 'tp')), may hold values from -6 to 6
- gain: bfloat16 [2048], replicated, may hold values from 0.099609375 to 1.8984375
- routes: int32 [8192, 4], P('sp'), may hold values from 0 to 63, all different within a row; in each aligned block of 16 rows (0 to 15, 16 to 31, ...) at most 2 rows name the same one
- route_weights: float32 [8192, 4], P('sp'), may hold values from 0.2 to 1
- w_gate: bfloat16 [64, 1024, 2048], P('sp', 'tp'), may hold values from -0.125 to 0.125
- w_up: bfloat16 [64, 1024, 2048], P('sp', 'tp'), may hold values from -0.125 to 0.125
- w_down: bfloat16 [64, 1024, 2048], P('sp', None, 'tp'), may hold values from -0.1875 to 0.1875
- shared_gate: bfloat16 [1024, 2048], P('tp'), may hold values from -0.125 to 0.125
- shared_up: bfloat16 [1024, 2048], P('tp'), may hold values from -0.125 to 0.125
- shared_down: bfloat16 [1024, 2048], P(None, 'tp'), may hold values from -0.1875 to 0.1875
Outputs:
- layer_out: bfloat16 [8192, 2048], P('sp', 'tp')
Inputs may be any that keep to these rules, and one draw needn't show every extreme that they name: `routes`: in each aligned block of 16 rows no expert is named in more than 2 rows, and some blocks reach 2; a row names 4 different experts.
All inputs are finite; a program needn't handle non-finite values.
Results may differ from a plain program's by a relative error of at most 0.014.
Values may be sent and summed in bfloat16 or wider, within the bound.
A program may use at most 64 MiB of HBM per device.

v0:
```python
import jax
import jax.numpy as jnp
from jax import lax
from jax.sharding import PartitionSpec as P

D = 2048
HEADS = 16
KV_HEADS = 4
HD = 64
WINDOW = 128
EXPERTS = 64
TOPK = 4
NORM_EPS = 1e-05


def with_halo(array, sides, width):
    for axis, dim in sides:
        devices, length = (lax.axis_size(axis), array.shape[dim])
        up = [(i, (i + 1) % devices) for i in range(devices - 1)]
        down = [(j, i) for i, j in up]
        last = lax.slice_in_dim(array, length - width, length, axis=dim)
        leading = lax.slice_in_dim(array, 0, width, axis=dim)
        before = lax.ppermute(last, axis, up)
        after = lax.ppermute(leading, axis, down)
        array = jnp.concatenate([before, array, after], axis=dim)
    return array


def laid_out(tiles, dim):
    tiles = jnp.moveaxis(tiles, 0, dim)
    dims = tiles.shape
    return tiles.reshape(*dims[:dim], dims[dim] * dims[dim + 1], *dims[dim + 2 :])


def from_everyone(array, axis):
    copies = jnp.broadcast_to(array, (lax.axis_size(axis), *array.shape))
    return lax.all_to_all(copies, axis, split_axis=0, concat_axis=0, tiled=True)


def gathered_copies(array, axis, dim):
    return laid_out(from_everyone(array, axis), dim)


def taken_together(array, axis):
    return from_everyone(array, axis).sum(axis=0)


def gather_turned(arrays, axis, dims):
    turned = [jnp.moveaxis(a, dim, 0) for a, dim in zip(arrays, dims)]
    widths = [t[0].size for t in turned]
    both = jnp.concatenate([t.reshape(-1, w) for t, w in zip(turned, widths)], axis=1)
    result = lax.all_gather(both, axis, axis=0, tiled=True)
    tiles = jnp.split(result, [sum(widths[:k]) for k in range(1, len(widths))], axis=1)
    return tuple(
        (
            jnp.moveaxis(b.reshape(-1, *t.shape[1:]), 0, dim)
            for b, t, dim in zip(tiles, turned, dims)
        )
    )


def slot_ids(block_routes, capacity):
    flat_routes = block_routes.reshape(-1)
    hit_table = (flat_routes[:, None] == jnp.arange(EXPERTS)[None, :]).astype(jnp.int32)
    earlier = jnp.cumsum(hit_table, axis=0) - hit_table
    slot_rank = jnp.sum(earlier * hit_table, axis=1)
    return flat_routes * capacity + slot_rank


def local(
    queries,
    keys,
    values,
    sink,
    w_out,
    stream,
    gain,
    routes,
    route_weights,
    w_gate,
    w_up,
    w_down,
    shared_gate,
    shared_up,
    shared_down,
):
    tok_dev = queries.shape[0]
    n_tp = lax.axis_size("tp")
    n_sp = lax.axis_size("sp")
    tp_idx = lax.axis_index("tp")
    sp_idx = lax.axis_index("sp")
    heads_dev = HEADS // n_tp
    group = HEADS // KV_HEADS
    kv_head = tp_idx * heads_dev // group
    key_own = lax.dynamic_slice_in_dim(keys, kv_head * HD, HD, 1)
    value_own = lax.dynamic_slice_in_dim(values, kv_head * HD, HD, 1)
    paired = jnp.concatenate([key_own, value_own], axis=1)
    padded = with_halo(paired, (("sp", 0),), WINDOW)
    blocks = tok_dev // WINDOW
    framed = padded.reshape(blocks + 2, WINDOW, 2 * HD)
    banded = jnp.concatenate([framed[:-2], framed[1:-1], framed[2:]], axis=1)
    key_band = banded[:, :, :HD]
    value_band = banded[:, :, HD:]
    query_blocks = queries.reshape(blocks, WINDOW, heads_dev, HD)
    scores = jnp.einsum(
        "nqhd,njd->nhqj", query_blocks, key_band, preferred_element_type=jnp.float32
    ) * HD ** (-0.5)
    offset = sp_idx * tok_dev
    seq_total = tok_dev * n_sp
    query_pos = (
        offset + jnp.arange(blocks)[:, None, None] * WINDOW + jnp.arange(WINDOW)[None, :, None]
    )
    key_pos = (
        offset
        - WINDOW
        + jnp.arange(blocks)[:, None, None] * WINDOW
        + jnp.arange(3 * WINDOW)[None, None, :]
    )
    allowed = (jnp.abs(query_pos - key_pos) <= WINDOW) & (key_pos >= 0) & (key_pos < seq_total)
    scores = jnp.where(allowed[:, None], scores, -jnp.inf)
    sink_level = sink.reshape(1, heads_dev, 1, 1)
    row_peak = jnp.maximum(scores.max(-1, keepdims=True), sink_level)
    probabilities = jnp.exp(scores - row_peak)
    denominator = probabilities.sum(-1, keepdims=True) + jnp.exp(sink_level - row_peak)
    weights = (probabilities / denominator).astype(jnp.bfloat16)
    attended = jnp.einsum("nhqj,njd->nqhd", weights, value_band, preferred_element_type=jnp.float32)
    attended = attended.astype(jnp.bfloat16).reshape(tok_dev, heads_dev * HD)
    rows_dev = tok_dev // n_tp
    d_dev = w_down.shape[2]
    all_heads = gathered_copies(attended, "tp", 1)
    w_cols, stream_cols = (
        lax.all_to_all(w_out, "tp", split_axis=1, concat_axis=0, tiled=True),
        lax.all_to_all(stream, "tp", split_axis=1, concat_axis=0, tiled=True),
    )
    projected = jnp.dot(all_heads, w_cols, preferred_element_type=jnp.float32)
    mixed_cols = (stream_cols.astype(jnp.float32) + projected).astype(jnp.bfloat16)
    residual = mixed_cols.astype(jnp.float32)
    square_sum = taken_together(jnp.sum(residual * residual, axis=-1), "tp")
    scale_rows = lax.rsqrt(square_sum[:, None] / D + NORM_EPS)
    gain_cols = lax.dynamic_slice_in_dim(gain, tp_idx * d_dev, d_dev, 0).astype(jnp.float32)
    normed_cols = (residual * scale_rows * gain_cols[None, :]).astype(jnp.bfloat16)
    normed = gathered_copies(normed_cols, "tp", 1)
    exp_dev = w_gate.shape[0]
    capacity = max(1, 2 * tok_dev * TOPK // (n_tp * EXPERTS))
    slot_count = EXPERTS * capacity
    blocked_routes = routes.reshape(n_tp, rows_dev, TOPK)
    destination = jax.vmap(lambda block_routes: slot_ids(block_routes, capacity))(blocked_routes)
    slot_select = destination[:, None, :] == jnp.arange(slot_count)[None, :, None]
    slot_select = slot_select.reshape(n_tp, slot_count, rows_dev, TOPK).astype(jnp.float32)
    dispatch_table = jnp.sum(slot_select, axis=-1).astype(jnp.bfloat16)
    combine_table = jnp.sum(slot_select * route_weights.reshape(n_tp, 1, rows_dev, TOPK), axis=-1)
    normed_blocks = normed.reshape(n_tp, rows_dev, D)
    own_table = lax.dynamic_index_in_dim(dispatch_table, tp_idx, 0, keepdims=False)
    own_rows = lax.dynamic_index_in_dim(normed_blocks, tp_idx, 0, keepdims=False)
    outgoing = jnp.dot(own_table, own_rows, preferred_element_type=jnp.float32).astype(jnp.bfloat16)
    arrived = lax.all_to_all(outgoing, "sp", split_axis=0, concat_axis=0, tiled=True)
    arrived = arrived.reshape(1, n_sp, exp_dev, capacity, D)
    piece_rows = lax.all_gather(arrived, "tp", axis=0, tiled=True)
    gate_act = jnp.einsum(
        "tsecd,efd->tsecf", piece_rows, w_gate, preferred_element_type=jnp.float32
    )
    up_act = jnp.einsum("tsecd,efd->tsecf", piece_rows, w_up, preferred_element_type=jnp.float32)
    hidden = (jax.nn.silu(gate_act) * up_act).astype(jnp.bfloat16)
    shared_gate_act = jnp.einsum(
        "td,fd->tf", normed, shared_gate, preferred_element_type=jnp.float32
    )
    shared_up_act = jnp.einsum("td,fd->tf", normed, shared_up, preferred_element_type=jnp.float32)
    shared_hidden = (jax.nn.silu(shared_gate_act) * shared_up_act).astype(jnp.bfloat16)
    shared_hidden = shared_hidden.reshape(1, 1, 1, tok_dev, shared_hidden.shape[1])
    expert_piece, shared_piece = gather_turned((hidden, shared_hidden), "tp", (4, 4))
    piece_width = expert_piece.shape[4]
    routed_total = jnp.einsum(
        "tsecf,efd->tsecd", expert_piece, w_down, preferred_element_type=jnp.float32
    )
    shared_total = jnp.dot(
        shared_piece.reshape(tok_dev, piece_width), shared_down, preferred_element_type=jnp.float32
    )
    returned = lax.all_to_all(
        routed_total.astype(jnp.bfloat16), "sp", split_axis=1, concat_axis=1, tiled=True
    )
    returned = returned.reshape(n_tp, slot_count, d_dev).astype(jnp.float32)
    routed = jnp.einsum("tmr,tmd->trd", combine_table, returned)
    routed = routed.reshape(tok_dev, d_dev)
    return (residual + routed + shared_total).astype(jnp.bfloat16)


def solution(mesh):
    placed = (
        P("sp", "tp"),
        P("sp", None),
        P("sp", None),
        P("tp"),
        P("tp", None),
        P(("sp", "tp"), None),
        P(),
        P("sp", None),
        P("sp", None),
        P("sp", "tp", None),
        P("sp", "tp", None),
        P("sp", None, "tp"),
        P("tp", None),
        P("tp", None),
        P(None, "tp"),
    )
    return jax.shard_map(
        local, mesh=mesh, in_specs=placed, out_specs=P("sp", "tp"), check_vma=False
    )
```

profile of v0, /device:TPU:8, one launch (start us, length us, event | category | flops | bytes accessed | tf_op | source)
XLA Modules:
  0.0 313.8 jit_solution(5770819059560762188)
XLA Ops:
  6.5 1.5 copy_bitcast_fusion.1
  8.1 9.1 %all-to-all-start = ((bf16[16,16,128]{2,0,1:T(8,128)(2,1)}), bf16[16,16,128]{2,0,1:T(8,128)(2,1)S(1)}, u32[]{:S(2)}, u32[]{:S(2)}) async-start(bf16[16,16,128]{2,0,1:T(8,128)(2,1)} %copy_bitcast_fusion.1), calls=%async_computation | async-start | bytes 131072 | tf_op jit(solution)/shard_map/all_to_all | solution.py:133
  17.2 1.0 constant_dynamic-slice_fusion
  18.2 1.9 collective-permute-start
  20.1 1.3 collective-permute-start.1
  21.6 1.7 copy_bitcast_fusion
  24.1 1.9 collective-permute-done.1
  26.5 1.3 fusion.51
  27.8 7.2 %all-to-all-start.2 = ((bf16[64,16,128]{2,0,1:T(8,128)(2,1)}), bf16[64,16,128]{2,0,1:T(8,128)(2,1)S(1)}, u32[]{:S(2)}, u32[]{:S(2)}) async-start(bf16[64,16,128]{2,0,1:T(8,128)(2,1)} %copy_bitcast_fusion), calls=%async_computation.2 | async-start | bytes 524288 | tf_op jit(solution)/shard_map/all_to_all | solution.py:132
  35.2 0.2 fusion.19
  35.4 9.2 %all-to-all-done.2 = bf16[64,16,128]{2,0,1:T(8,128)(2,1)S(1)} async-done(((bf16[64,16,128]{2,0,1:T(8,128)(2,1)}), bf16[64,16,128]{2,0,1:T(8,128)(2,1)S(1)}, u32[]{:S(2)}, u32[]{:S(2)}) %all-to-all-start.2) | async-done | bytes 262176 | tf_op jit(solution)/shard_map/all_to_all | solution.py:132
  44.7 0.8 broadcast_in_dim.11
  45.5 5.0 %all-to-all-start.1 = ((bf16[16,256,64]{1,2,0:T(8,128)(2,1)}), bf16[16,256,64]{1,2,0:T(8,128)(2,1)S(1)}, u32[]{:S(2)}, u32[]{:S(2)}) async-start(bf16[16,256,64]{1,2,0:T(8,128)(2,1)} %broadcast_in_dim.11), calls=%async_computation.1 | async-start | bytes 1048576 | tf_op jit(solution)/shard_map/all_to_all | solution.py:37
  50.7 14.4 %all-to-all-done.1 = bf16[16,256,64]{1,2,0:T(8,128)(2,1)S(1)} async-done(((bf16[16,256,64]{1,2,0:T(8,128)(2,1)}), bf16[16,256,64]{1,2,0:T(8,128)(2,1)S(1)}, u32[]{:S(2)}, u32[]{:S(2)}) %all-to-all-start.1) | async-done | bytes 524320 | tf_op jit(solution)/shard_map/all_to_all | solution.py:37
  65.1 0.3 multiply_reduce_fusion
  65.4 0.6 broadcast_in_dim.12
  66.0 5.7 %all-to-all-start.3 = ((f32[16,1,256]{2,1,0:T(1,128)}), f32[16,1,256]{2,1,0:T(1,128)S(1)}, u32[]{:S(2)}, u32[]{:S(2)}) async-start(f32[16,1,256]{2,1,0:T(1,128)} %broadcast_in_dim.12), calls=%async_computation.3 | async-start | bytes 32768 | tf_op jit(solution)/shard_map/all_to_all | solution.py:37
  71.7 0.8 dynamic-slice_convert_fusion.1
  72.4 5.5 %all-to-all-done.3 = f32[16,1,256]{2,1,0:T(1,128)S(1)} async-done(((f32[16,1,256]{2,1,0:T(1,128)}), f32[16,1,256]{2,1,0:T(1,128)S(1)}, u32[]{:S(2)}, u32[]{:S(2)}) %all-to-all-start.3) | async-done | bytes 16416 | tf_op jit(solution)/shard_map/all_to_all | solution.py:37
  78.1 1.1 broadcast_in_dim.13
  79.2 4.9 %all-to-all-start.4 = ((bf16[16,256,128]{1,2,0:T(8,128)(2,1)}), bf16[16,256,128]{1,2,0:T(8,128)(2,1)S(1)}, u32[]{:S(2)}, u32[]{:S(2)}) async-start(bf16[16,256,128]{1,2,0:T(8,128)(2,1)} %broadcast_in_dim.13), calls=%async_computation.4 | async-start | bytes 2097152 | tf_op jit(solution)/shard_map/all_to_all | solution.py:37
  84.7 1.4 select_reduce_fusion.1
  86.2 1.0 select_reduce_fusion
  87.2 21.5 %all-to-all-done.4 = bf16[16,256,128]{1,2,0:T(8,128)(2,1)S(1)} async-done(((bf16[16,256,128]{1,2,0:T(8,128)(2,1)}), bf16[16,256,128]{1,2,0:T(8,128)(2,1)S(1)}, u32[]{:S(2)}, u32[]{:S(2)}) %all-to-all-start.4) | async-done | bytes 1048608 | tf_op jit(solution)/shard_map/all_to_all | solution.py:37
  108.7 1.1 copy.141
  109.8 1.3 reshape_reshape.2
  111.1 1.2 convolution_convert_fusion
  112.2 0.2 all_to_all.49
  112.4 33.3 %all_to_all.59 = bf16[32,4,2048]{2,1,0:T(4,128)(2,1)S(1)} all-to-all(bf16[32,4,2048]{2,1,0:T(4,128)(2,1)S(1)} %all_to_all.49), channel_id=1, replica_groups=mesh['sp'=32,'tp'=16] {'sp'}, dimensions={0} | all-to-all | bytes 1048576 | tf_op jit(solution)/shard_map/all_to_all | solution.py:156
  145.7 1.1 copy.142
  146.8 0.2 all-gather.5.cloned.1.call-start
  147.1 0.3 fusion.52
  147.4 1.2 fusion.18
  148.8 50.0 %all-gather.3.cloned.1.call-done = bf16[16,32,2,2,2048]{4,1,3,0,2:T(8,128)(2,1)} async-done(((bf16[1,32,2,2,2048]{4,1,3,0,2:T(8,128)(2,1)}), bf16[16,32,2,2,2048]{4,1,3,0,2:T(8,128)(2,1)}) %all-gather.3.cloned.1.call-update) | async-done | bytes 8388624 | tf_op jit(solution)/shard_map/all_gather | solution.py:158
  198.8 5.8 %convolution_bitcast_fusion.1 = f32[64,16,32,2,2]{0,2,4,1,3:T(8,128)S(1)} fusion(bf16[16,32,2,2,2048]{4,1,3,0,2:T(8,128)(2,1)} %all-gather.3.cloned.1.call-done, bf16[2,64,2048]{2,1,0:T(8,128)(2,1)S(1)} %copy-done.2), kind=kOutput, calls=%fused_computation.6 | convolution fusion | flops 536870912 | bytes 9437184 | tf_op jit(solution)/shard_map/tsecd,efd->tsecf/dot_general | solution.py:159
  204.7 2.3 fusion.4
  207.0 0.5 copy.143
  207.6 1.0 copy.145
  208.6 44.9 %all-gather.5.cloned.1.call-done = bf16[1024,2304]{1,0:T(8,128)(2,1)} async-done(((bf16[64,2304]{1,0:T(8,128)(2,1)}), bf16[1024,2304]{1,0:T(8,128)(2,1)}) %all-gather.5.cloned.1.call-update) | async-done | bytes 4718608 | tf_op jit(solution)/shard_map/all_gather | solution.py:52
  253.5 4.8 %split.8 = bf16[1024,2048]{1,0:T(8,128)(2,1)} slice(bf16[1024,2304]{1,0:T(8,128)(2,1)} %all-gather.5.cloned.1.call-done), slice={[0:1024], [0:2048]} | slice | bytes 8388608 | tf_op jit(solution)/shard_map/split | solution.py:53
  258.3 6.5 %copy.146 = bf16[1024,2048]{0,1:T(8,128)(2,1)} copy(bf16[1024,2048]{1,0:T(8,128)(2,1)} %split.8) | data formatting | bytes 8388608 | tf_op jit(solution)/shard_map/split | solution.py:53
  264.8 7.2 %reshape.237 = bf16[1024,16,32,2,2]{0,4,3,2,1:T(2,128)(2,1)} reshape(bf16[1024,2048]{0,1:T(8,128)(2,1)} %copy.146) | data formatting | bytes 8388608 | tf_op jit(solution)/shard_map/reshape | solution.py:56
  272.0 3.6 %fusion.8 = bf16[16,32,2,2,128]{4,1,3,0,2:T(8,128)(2,1)S(1)} fusion(bf16[1024,16,32,2,2]{0,4,3,2,1:T(2,128)(2,1)} %reshape.237, bf16[2,1024,128]{2,1,0:T(8,128)(2,1)S(1)} %copy-done), kind=kOutput, calls=%fused_computation.9 | convolution fusion | flops 537133056 | bytes 5242880 | tf_op jit(solution)/shard_map/tsecf,efd->tsecd/dot_general | solution.py:172
  275.6 0.5 copy.148
  276.2 28.2 %all_to_all.60 = bf16[16,32,2,2,128]{4,3,0,2,1:T(2,128)(2,1)S(1)} all-to-all(bf16[16,32,2,2,128]{4,3,0,2,1:T(2,128)(2,1)S(1)} %copy.148), channel_id=1, replica_groups=mesh['sp'=32,'tp'=16] {'sp'}, dimensions={1} | all-to-all | bytes 1048576 | tf_op jit(solution)/shard_map/all_to_all | solution.py:178
  304.5 0.3 fusion.28
  304.9 1.3 fusion.16
  306.2 0.7 copy.153
  (58 shorter events, 2.4 us)
Async XLA Ops:
  6.5 265.5 %copy-start = (bf16[2,1024,128]{2,1,0:T(8,128)(2,1)S(1)}, bf16[2,1024,128]{2,1,0:T(8,128)(2,1)}, u32[]{:S(2)}) copy-start(bf16[2,1024,128]{2,1,0:T(8,128)(2,1)} %param.26) | copy-start | bytes 1572868
  8.1 19.8 %all-to-all-start = ((bf16[16,16,128]{2,0,1:T(8,128)(2,1)}), bf16[16,16,128]{2,0,1:T(8,128)(2,1)S(1)}, u32[]{:S(2)}, u32[]{:S(2)}) async-start(bf16[16,16,128]{2,0,1:T(8,128)(2,1)} %copy_bitcast_fusion.1), calls=%async_computation | async-start | bytes 131072 | tf_op jit(solution)/shard_map/all_to_all | solution.py:133
  18.2 5.8 %collective-permute-start = (bf16[128,128]{1,0:T(8,128)(2,1)S(1)}, bf16[128,128]{1,0:T(8,128)(2,1)S(1)}, u32[]{:S(2)}, u32[]{:S(2)}) collective-permute-start(bf16[128,128]{1,0:T(8,128)(2,1)S(1)} %get-tuple-element.10), channel_id=1, source_target_pairs={{0,16},{16,32},{32,48},{48,64},{64,80},{80,96},{96,112},{112,128},... | collective-permute-start | bytes 98312 | tf_op jit(solution)/shard_map/ppermute | solution.py:23
  20.1 5.8 %collective-permute-start.1 = (bf16[128,128]{1,0:T(8,128)(2,1)S(1)}, bf16[128,128]{1,0:T(8,128)(2,1)S(1)}, u32[]{:S(2)}, u32[]{:S(2)}) collective-permute-start(bf16[128,128]{1,0:T(8,128)(2,1)S(1)} %get-tuple-element.11), channel_id=1, source_target_pairs={{16,0},{32,16},{48,32},{64,48},{80,64},{96,80},{112,96},{128,112},... | collective-permute-start | bytes 98312 | tf_op jit(solution)/shard_map/ppermute | solution.py:24
  27.8 56.3 %copy-start.6 = (s32[256,4]{0,1:T(4,128)S(1)}, s32[256,4]{0,1:T(4,128)}, u32[]{:S(2)}) copy-start(s32[256,4]{0,1:T(4,128)} %param.22) | copy-start | bytes 12292
  27.8 56.5 %copy-start.7 = (f32[256,4]{0,1:T(4,128)S(1)}, f32[256,4]{0,1:T(4,128)}, u32[]{:S(2)}) copy-start(f32[256,4]{0,1:T(4,128)} %param.23) | copy-start | bytes 12292
  27.8 16.8 %all-to-all-start.2 = ((bf16[64,16,128]{2,0,1:T(8,128)(2,1)}), bf16[64,16,128]{2,0,1:T(8,128)(2,1)S(1)}, u32[]{:S(2)}, u32[]{:S(2)}) async-start(bf16[64,16,128]{2,0,1:T(8,128)(2,1)} %copy_bitcast_fusion), calls=%async_computation.2 | async-start | bytes 524288 | tf_op jit(solution)/shard_map/all_to_all | solution.py:132
  45.5 19.5 %all-to-all-start.1 = ((bf16[16,256,64]{1,2,0:T(8,128)(2,1)}), bf16[16,256,64]{1,2,0:T(8,128)(2,1)S(1)}, u32[]{:S(2)}, u32[]{:S(2)}) async-start(bf16[16,256,64]{1,2,0:T(8,128)(2,1)} %broadcast_in_dim.11), calls=%async_computation.1 | async-start | bytes 1048576 | tf_op jit(solution)/shard_map/all_to_all | solution.py:37
  66.0 12.0 %all-to-all-start.3 = ((f32[16,1,256]{2,1,0:T(1,128)}), f32[16,1,256]{2,1,0:T(1,128)S(1)}, u32[]{:S(2)}, u32[]{:S(2)}) async-start(f32[16,1,256]{2,1,0:T(1,128)} %broadcast_in_dim.12), calls=%async_computation.3 | async-start | bytes 32768 | tf_op jit(solution)/shard_map/all_to_all | solution.py:37
  79.2 29.6 %all-to-all-start.4 = ((bf16[16,256,128]{1,2,0:T(8,128)(2,1)}), bf16[16,256,128]{1,2,0:T(8,128)(2,1)S(1)}, u32[]{:S(2)}, u32[]{:S(2)}) async-start(bf16[16,256,128]{1,2,0:T(8,128)(2,1)} %broadcast_in_dim.13), calls=%async_computation.4 | async-start | bytes 2097152 | tf_op jit(solution)/shard_map/all_to_all | solution.py:37
  84.1 114.7 %all-gather.3.cloned.1.call-start = ((), (), s32[]{:S(2)}) async-start(), calls=%async_computation.7 | async-start | bytes 8912896 | tf_op jit(solution)/shard_map/all_gather | solution.py:158
  84.1 63.0 %copy-start.4 = (bf16[64,2048]{1,0:T(8,128)(2,1)S(1)}, bf16[64,2048]{1,0:T(8,128)(2,1)}, u32[]{:S(2)}) copy-start(bf16[64,2048]{1,0:T(8,128)(2,1)} %param.27) | copy-start | bytes 786436
  109.8 89.0 %copy-start.2 = (bf16[2,64,2048]{2,1,0:T(8,128)(2,1)S(1)}, bf16[2,64,2048]{2,1,0:T(8,128)(2,1)}, u32[]{:S(2)}) copy-start(bf16[2,64,2048]{2,1,0:T(8,128)(2,1)} %param.24) | copy-start | bytes 1572868
  146.8 106.7 %all-gather.5.cloned.1.call-start = ((), (), s32[]{:S(2)}) async-start(), calls=%async_computation.8 | async-start | bytes 5013504 | tf_op jit(solution)/shard_map/all_gather | solution.py:52
  148.8 55.9 %copy-start.8 = (bf16[2,64,2048]{2,1,0:T(8,128)(2,1)S(1)}, bf16[2,64,2048]{2,1,0:T(8,128)(2,1)}, u32[]{:S(2)}) copy-start(bf16[2,64,2048]{2,1,0:T(8,128)(2,1)} %param.25) | copy-start | bytes 1572868
  198.8 5.9 %copy-start.1 = (bf16[16,32,2,2,2048]{4,1,3,0,2:T(8,128)(2,1)S(1)}, bf16[16,32,2,2,2048]{4,1,3,0,2:T(8,128)(2,1)}, u32[]{:S(2)}) copy-start(bf16[16,32,2,2,2048]{4,1,3,0,2:T(8,128)(2,1)} %all-gather.3.cloned.1.call-done) | copy-start | bytes 25165828
  272.0 32.5 %copy-start.5 = (bf16[16,128,16]{1,2,0:T(8,128)(2,1)S(1)}, bf16[16,128,16]{1,2,0:T(8,128)(2,1)}, u32[]{:S(2)}) copy-start(bf16[16,128,16]{1,2,0:T(8,128)(2,1)} %get-tuple-element.5) | copy-start | bytes 196612
  272.0 32.8 %copy-start.3 = (bf16[1024,128]{1,0:T(8,128)(2,1)S(1)}, bf16[1024,128]{1,0:T(8,128)(2,1)}, u32[]{:S(2)}) copy-start(bf16[1024,128]{1,0:T(8,128)(2,1)} %param.29) | copy-start | bytes 786436
Sparse Core Ops, SparseCore 0:
  147.0 51.7 all-gather.2
  208.7 44.7 all-gather.4
where the time goes:
time: 315 us; the launch traced here: 314 us
  waiting for transfers between devices  147 us (47%)
  blocking collectives  61.5 us (20%)
  starting transfers between devices  35.4 us (11%)
  local copies, waits for them, and re-layouts  33.1 us (11%)
  matrix products  17.8 us (6%)
  between operations  14.5 us (5%)
  other arithmetic  4.01 us (1%)
    all_gather x1, waiting for transfers between devices, local(): piece_rows = lax.all_gather(arrived, 'tp', axis=0, tiled=True)  50 us
    all_gather x1, waiting for transfers between devices, gather_turned(): result = lax.all_gather(both, axis, axis=0, tiled=True)  44.9 us
    all_to_all x3, waiting for transfers between devices, from_everyone(): return lax.all_to_all(copies, axis, split_axis=0, concat_axis=0, tiled=True)  41.4 us
    all_to_all x1, blocking collectives, local(): lax.all_to_all(outgoing, 'sp', split_axis=0, concat_axis=0, tiled=True)  33.3 us
    all_to_all x1, blocking collectives, local(): lax.all_to_all(routed_total.astype(jnp.bfloat16), 'sp', split_axis=1, con...  28.2 us
    all_to_all x3, starting transfers between devices, from_everyone(): return lax.all_to_all(copies, axis, split_axis=0, concat_axis=0, tiled=True)  15.6 us
    split x2, local copies, waits for them, and re-layouts, gather_turned(): jnp.split(result, [sum(widths[:k]) for k in range(1, len(widths))], axis=1)  11.3 us
    all_to_all x1, waiting for transfers between devices, local(): lax.all_to_all(w_out, 'tp', split_axis=1, concat_axis=0, tiled=True)  9.24 us
  transfers between devices with their start and end apart: 9, of which 7 were waited for; matrix products, arithmetic and copies ran while one was open for 3% of the time, Pallas kernels for 0%

commit v1 on v0

--- a/solution.py
+++ b/solution.py
@@ -11,6 +11,12 @@
 EXPERTS = 64
 TOPK = 4
 NORM_EPS = 1e-05
+
+
+def exchange_blocks(x, mesh_axis, split, join):
+    cells = jnp.split(x, lax.axis_size(mesh_axis), axis=split)
+    received = lax.all_to_all(jnp.stack(cells), mesh_axis, 0, 0)
+    return jnp.concatenate(received, axis=join)
 
 
 def with_halo(array, sides, width):
@@ -129,7 +135,7 @@
     d_dev = w_down.shape[2]
     all_heads = gathered_copies(attended, "tp", 1)
     w_cols, stream_cols = (
-        lax.all_to_all(w_out, "tp", split_axis=1, concat_axis=0, tiled=True),
+        exchange_blocks(w_out, "tp", 1, 0),
         lax.all_to_all(stream, "tp", split_axis=1, concat_axis=0, tiled=True),
     )
     projected = jnp.dot(all_heads, w_cols, preferred_element_type=jnp.float32)

time: 315 us -> 333 us (1.057)
  local copies, waits for them, and re-layouts: 33.1 us -> 52.5 us
    unnamed x20 -> x35, local copies, waits for them, and re-layouts: 0.19 us -> 20 us
  transfers between devices with their start and end apart: 9 -> 9, of which waited for: 7 -> 6; matrix products, arithmetic and copies ran while one was open for 3% -> 9% of each run, Pallas kernels for 0% -> 0%
where the time goes in v1:
time: 333 us; the launch traced here: 331 us
  waiting for transfers between devices  146 us (44%)
  blocking collectives  61.4 us (18%)
  local copies, waits for them, and re-layouts  52.5 us (16%)
  starting transfers between devices  35.4 us (11%)
  matrix products  17.8 us (5%)
  between operations  14.5 us (4%)
  other arithmetic  4.01 us (1%)
    all_gather x1, waiting for transfers between devices, local(): piece_rows = lax.all_gather(arrived, 'tp', axis=0, tiled=True)  50 us
    all_gather x1, waiting for transfers between devices, gather_turned(): result = lax.all_gather(both, axis, axis=0, tiled=True)  44.9 us
    all_to_all x3, waiting for transfers between devices, from_everyone(): return lax.all_to_all(copies, axis, split_axis=0, concat_axis=0, tiled=True)  41.4 us
    all_to_all x1, blocking collectives, local(): lax.all_to_all(outgoing, 'sp', split_axis=0, concat_axis=0, tiled=True)  33.2 us
    all_to_all x1, blocking collectives, local(): lax.all_to_all(routed_total.astype(jnp.bfloat16), 'sp', split_axis=1, con...  28.2 us
    unnamed x35, local copies, waits for them, and re-layouts  20 us
    all_to_all x3, starting transfers between devices, from_everyone(): return lax.all_to_all(copies, axis, split_axis=0, concat_axis=0, tiled=True)  15.6 us
    split x2, local copies, waits for them, and re-layouts, gather_turned(): jnp.split(result, [sum(widths[:k]) for k in range(1, len(widths))], axis=1)  11.3 us
  transfers between devices with their start and end apart: 9, of which 6 were waited for; matrix products, arithmetic and copies ran while one was open for 9% of the time, Pallas kernels for 0%

profile of v1, /device:TPU:8, one launch (start us, length us, event | category | flops | bytes accessed | tf_op | source)
XLA Modules:
  0.0 331.2 jit_solution(11646071065068909664)
XLA Ops:
  6.5 1.5 copy_bitcast_fusion
  8.1 9.1 %all-to-all-start = ((bf16[16,16,128]{2,0,1:T(8,128)(2,1)}), bf16[16,16,128]{2,0,1:T(8,128)(2,1)S(1)}, u32[]{:S(2)}, u32[]{:S(2)}) async-start(bf16[16,16,128]{2,0,1:T(8,128)(2,1)} %copy_bitcast_fusion), calls=%async_computation | async-start | bytes 131072 | tf_op jit(solution)/shard_map/all_to_all | solution.py:139
  18.2 1.9 collective-permute-start
  20.1 1.3 collective-permute-start.1
  21.6 1.3 constant_dynamic-update-slice_fusion.15
  22.9 1.3 constant_dynamic-update-slice_fusion.14
  24.2 1.3 constant_dynamic-update-slice_fusion.13
  25.6 1.3 constant_dynamic-update-slice_fusion.12
  26.9 1.3 constant_dynamic-update-slice_fusion.11
  28.2 1.3 constant_dynamic-update-slice_fusion.10
  29.5 1.3 constant_dynamic-update-slice_fusion.9
  30.8 1.3 constant_dynamic-update-slice_fusion.8
  32.1 1.3 constant_dynamic-update-slice_fusion.7
  33.5 1.3 constant_dynamic-update-slice_fusion.6
  34.8 1.3 constant_dynamic-update-slice_fusion.5
  36.1 1.3 constant_dynamic-update-slice_fusion.4
  37.4 1.3 constant_dynamic-update-slice_fusion.3
  38.7 1.3 constant_dynamic-update-slice_fusion.2
  40.1 1.3 constant_dynamic-update-slice_fusion.1
  41.4 1.3 constant_dynamic-update-slice_fusion
  44.0 1.3 fusion.50
  45.4 7.2 %all-to-all-start.2 = ((bf16[16,64,128]{2,1,0:T(8,128)(2,1)}), bf16[16,64,128]{2,1,0:T(8,128)(2,1)S(1)}, u32[]{:S(2)}, u32[]{:S(2)}) async-start(bf16[16,64,128]{2,1,0:T(8,128)(2,1)} %constant_dynamic-update-slice_fusion), calls=%async_computation.2 | async-start | bytes 524288 | tf_op jit(solution)/shard_map/all_to_all | solution.py:18
  53.0 9.2 %all-to-all-done.2 = bf16[16,64,128]{2,1,0:T(8,128)(2,1)S(1)} async-done(((bf16[16,64,128]{2,1,0:T(8,128)(2,1)}), bf16[16,64,128]{2,1,0:T(8,128)(2,1)S(1)}, u32[]{:S(2)}, u32[]{:S(2)}) %all-to-all-start.2) | async-done | bytes 262176 | tf_op jit(solution)/shard_map/all_to_all | solution.py:18
  63.0 5.0 %all-to-all-start.1 = ((bf16[16,256,64]{1,2,0:T(8,128)(2,1)}), bf16[16,256,64]{1,2,0:T(8,128)(2,1)S(1)}, u32[]{:S(2)}, u32[]{:S(2)}) async-start(bf16[16,256,64]{1,2,0:T(8,128)(2,1)} %broadcast_in_dim.11), calls=%async_computation.1 | async-start | bytes 1048576 | tf_op jit(solution)/shard_map/all_to_all | solution.py:43
  68.2 14.4 %all-to-all-done.1 = bf16[16,256,64]{1,2,0:T(8,128)(2,1)S(1)} async-done(((bf16[16,256,64]{1,2,0:T(8,128)(2,1)}), bf16[16,256,64]{1,2,0:T(8,128)(2,1)S(1)}, u32[]{:S(2)}, u32[]{:S(2)}) %all-to-all-start.1) | async-done | bytes 524320 | tf_op jit(solution)/shard_map/all_to_all | solution.py:43
  83.5 5.7 %all-to-all-start.3 = ((f32[16,1,256]{2,1,0:T(1,128)}), f32[16,1,256]{2,1,0:T(1,128)S(1)}, u32[]{:S(2)}, u32[]{:S(2)}) async-start(f32[16,1,256]{2,1,0:T(1,128)} %broadcast_in_dim.12), calls=%async_computation.3 | async-start | bytes 32768 | tf_op jit(solution)/shard_map/all_to_all | solution.py:43
  89.9 5.5 %all-to-all-done.3 = f32[16,1,256]{2,1,0:T(1,128)S(1)} async-done(((f32[16,1,256]{2,1,0:T(1,128)}), f32[16,1,256]{2,1,0:T(1,128)S(1)}, u32[]{:S(2)}, u32[]{:S(2)}) %all-to-all-start.3) | async-done | bytes 16416 | tf_op jit(solution)/shard_map/all_to_all | solution.py:43
  95.6 1.1 broadcast_in_dim.13
  96.7 4.9 %all-to-all-start.4 = ((bf16[16,256,128]{1,2,0:T(8,128)(2,1)}), bf16[16,256,128]{1,2,0:T(8,128)(2,1)S(1)}, u32[]{:S(2)}, u32[]{:S(2)}) async-start(bf16[16,256,128]{1,2,0:T(8,128)(2,1)} %broadcast_in_dim.13), calls=%async_computation.4 | async-start | bytes 2097152 | tf_op jit(solution)/shard_map/all_to_all | solution.py:43
  102.2 1.4 select_reduce_fusion.1
  103.7 1.0 select_reduce_fusion
  104.7 21.5 %all-to-all-done.4 = bf16[16,256,128]{1,2,0:T(8,128)(2,1)S(1)} async-done(((bf16[16,256,128]{1,2,0:T(8,128)(2,1)}), bf16[16,256,128]{1,2,0:T(8,128)(2,1)S(1)}, u32[]{:S(2)}, u32[]{:S(2)}) %all-to-all-start.4) | async-done | bytes 1048608 | tf_op jit(solution)/shard_map/all_to_all | solution.py:43
  126.2 1.1 copy.136
  127.3 1.3 reshape_reshape.2
  128.6 1.2 convolution_convert_fusion
  129.9 33.2 %all_to_all.48 = bf16[32,4,2048]{2,1,0:T(4,128)(2,1)S(1)} all-to-all(bf16[32,4,2048]{2,1,0:T(4,128)(2,1)S(1)} %all_to_all.38), channel_id=1, replica_groups=mesh['sp'=32,'tp'=16] {'sp'}, dimensions={0} | all-to-all | bytes 1048576 | tf_op jit(solution)/shard_map/all_to_all | solution.py:162
  163.2 1.1 copy.137
  164.9 1.2 fusion.18
  166.2 50.0 %all-gather.3.cloned.1.call-done = bf16[16,32,2,2,2048]{4,1,3,0,2:T(8,128)(2,1)} async-done(((bf16[1,32,2,2,2048]{4,1,3,0,2:T(8,128)(2,1)}), bf16[16,32,2,2,2048]{4,1,3,0,2:T(8,128)(2,1)}) %all-gather.3.cloned.1.call-update) | async-done | bytes 8388624 | tf_op jit(solution)/shard_map/all_gather | solution.py:164
  216.3 5.8 %convolution_bitcast_fusion.1 = f32[64,16,32,2,2]{0,2,4,1,3:T(8,128)S(1)} fusion(bf16[16,32,2,2,2048]{4,1,3,0,2:T(8,128)(2,1)} %all-gather.3.cloned.1.call-done, bf16[2,64,2048]{2,1,0:T(8,128)(2,1)S(1)} %copy-done.2), kind=kOutput, calls=%fused_computation.6 | convolution fusion | flops 536870912 | bytes 9437184 | tf_op jit(solution)/shard_map/tsecd,efd->tsecf/dot_general | solution.py:165
  222.1 2.3 fusion.4
  226.1 44.9 %all-gather.5.cloned.1.call-done = bf16[1024,2304]{1,0:T(8,128)(2,1)} async-done(((bf16[64,2304]{1,0:T(8,128)(2,1)}), bf16[1024,2304]{1,0:T(8,128)(2,1)}) %all-gather.5.cloned.1.call-update) | async-done | bytes 4718608 | tf_op jit(solution)/shard_map/all_gather | solution.py:58
  271.0 4.8 %split.72 = bf16[1024,2048]{1,0:T(8,128)(2,1)} slice(bf16[1024,2304]{1,0:T(8,128)(2,1)} %all-gather.5.cloned.1.call-done), slice={[0:1024], [0:2048]} | slice | bytes 8388608 | tf_op jit(solution)/shard_map/split | solution.py:59
  275.8 6.5 %copy.141 = bf16[1024,2048]{0,1:T(8,128)(2,1)} copy(bf16[1024,2048]{1,0:T(8,128)(2,1)} %split.72) | data formatting | bytes 8388608 | tf_op jit(solution)/shard_map/split | solution.py:59
  282.3 7.2 %reshape.235 = bf16[1024,16,32,2,2]{0,4,3,2,1:T(2,128)(2,1)} reshape(bf16[1024,2048]{0,1:T(8,128)(2,1)} %copy.141) | data formatting | bytes 8388608 | tf_op jit(solution)/shard_map/reshape | solution.py:62
  289.5 3.6 %fusion.8 = bf16[16,32,2,2,128]{4,1,3,0,2:T(8,128)(2,1)S(1)} fusion(bf16[1024,16,32,2,2]{0,4,3,2,1:T(2,128)(2,1)} %reshape.235, bf16[2,1024,128]{2,1,0:T(8,128)(2,1)S(1)} %copy-done), kind=kOutput, calls=%fused_computation.9 | convolution fusion | flops 537133056 | bytes 5242880 | tf_op jit(solution)/shard_map/tsecf,efd->tsecd/dot_general | solution.py:178
  293.6 28.2 %all_to_all.49 = bf16[16,32,2,2,128]{4,3,0,2,1:T(2,128)(2,1)S(1)} all-to-all(bf16[16,32,2,2,128]{4,3,0,2,1:T(2,128)(2,1)S(1)} %copy.143), channel_id=1, replica_groups=mesh['sp'=32,'tp'=16] {'sp'}, dimensions={1} | all-to-all | bytes 1048576 | tf_op jit(solution)/shard_map/all_to_all | solution.py:184
  322.3 1.3 fusion.16
  (73 shorter events, 9.8 us)
Async XLA Ops:
  6.5 283.0 %copy-start = (bf16[2,1024,128]{2,1,0:T(8,128)(2,1)S(1)}, bf16[2,1024,128]{2,1,0:T(8,128)(2,1)}, u32[]{:S(2)}) copy-start(bf16[2,1024,128]{2,1,0:T(8,128)(2,1)} %param.26) | copy-start | bytes 1572868
  8.1 37.3 %all-to-all-start = ((bf16[16,16,128]{2,0,1:T(8,128)(2,1)}), bf16[16,16,128]{2,0,1:T(8,128)(2,1)S(1)}, u32[]{:S(2)}, u32[]{:S(2)}) async-start(bf16[16,16,128]{2,0,1:T(8,128)(2,1)} %copy_bitcast_fusion), calls=%async_computation | async-start | bytes 131072 | tf_op jit(solution)/shard_map/all_to_all | solution.py:139
  18.2 25.2 %collective-permute-start = (bf16[128,128]{1,0:T(8,128)(2,1)S(1)}, bf16[128,128]{1,0:T(8,128)(2,1)S(1)}, u32[]{:S(2)}, u32[]{:S(2)}) collective-permute-start(bf16[128,128]{1,0:T(8,128)(2,1)S(1)} %get-tuple-element.10), channel_id=1, source_target_pairs={{0,16},{16,32},{32,48},{48,64},{64,80},{80,96},{96,112},{112,128},... | collective-permute-start | bytes 98312 | tf_op jit(solution)/shard_map/ppermute | solution.py:29
  20.1 23.3 %collective-permute-start.1 = (bf16[128,128]{1,0:T(8,128)(2,1)S(1)}, bf16[128,128]{1,0:T(8,128)(2,1)S(1)}, u32[]{:S(2)}, u32[]{:S(2)}) collective-permute-start(bf16[128,128]{1,0:T(8,128)(2,1)S(1)} %get-tuple-element.11), channel_id=1, source_target_pairs={{16,0},{32,16},{48,32},{64,48},{80,64},{96,80},{112,96},{128,112},... | collective-permute-start | bytes 98312 | tf_op jit(solution)/shard_map/ppermute | solution.py:30
  45.3 56.3 %copy-start.6 = (s32[256,4]{0,1:T(4,128)S(1)}, s32[256,4]{0,1:T(4,128)}, u32[]{:S(2)}) copy-start(s32[256,4]{0,1:T(4,128)} %param.22) | copy-start | bytes 12292
  45.3 56.6 %copy-start.7 = (f32[256,4]{0,1:T(4,128)S(1)}, f32[256,4]{0,1:T(4,128)}, u32[]{:S(2)}) copy-start(f32[256,4]{0,1:T(4,128)} %param.23) | copy-start | bytes 12292
  45.4 16.8 %all-to-all-start.2 = ((bf16[16,64,128]{2,1,0:T(8,128)(2,1)}), bf16[16,64,128]{2,1,0:T(8,128)(2,1)S(1)}, u32[]{:S(2)}, u32[]{:S(2)}) async-start(bf16[16,64,128]{2,1,0:T(8,128)(2,1)} %constant_dynamic-update-slice_fusion), calls=%async_computation.2 | async-start | bytes 524288 | tf_op jit(solution)/shard_map/all_to_all | solution.py:18
  63.0 19.5 %all-to-all-start.1 = ((bf16[16,256,64]{1,2,0:T(8,128)(2,1)}), bf16[16,256,64]{1,2,0:T(8,128)(2,1)S(1)}, u32[]{:S(2)}, u32[]{:S(2)}) async-start(bf16[16,256,64]{1,2,0:T(8,128)(2,1)} %broadcast_in_dim.11), calls=%async_computation.1 | async-start | bytes 1048576 | tf_op jit(solution)/shard_map/all_to_all | solution.py:43
  83.5 12.0 %all-to-all-start.3 = ((f32[16,1,256]{2,1,0:T(1,128)}), f32[16,1,256]{2,1,0:T(1,128)S(1)}, u32[]{:S(2)}, u32[]{:S(2)}) async-start(f32[16,1,256]{2,1,0:T(1,128)} %broadcast_in_dim.12), calls=%async_computation.3 | async-start | bytes 32768 | tf_op jit(solution)/shard_map/all_to_all | solution.py:43
  96.7 29.6 %all-to-all-start.4 = ((bf16[16,256,128]{1,2,0:T(8,128)(2,1)}), bf16[16,256,128]{1,2,0:T(8,128)(2,1)S(1)}, u32[]{:S(2)}, u32[]{:S(2)}) async-start(bf16[16,256,128]{1,2,0:T(8,128)(2,1)} %broadcast_in_dim.13), calls=%async_computation.4 | async-start | bytes 2097152 | tf_op jit(solution)/shard_map/all_to_all | solution.py:43
  101.6 114.7 %all-gather.3.cloned.1.call-start = ((), (), s32[]{:S(2)}) async-start(), calls=%async_computation.7 | async-start | bytes 8912896 | tf_op jit(solution)/shard_map/all_gather | solution.py:164
  101.6 62.9 %copy-start.4 = (bf16[64,2048]{1,0:T(8,128)(2,1)S(1)}, bf16[64,2048]{1,0:T(8,128)(2,1)}, u32[]{:S(2)}) copy-start(bf16[64,2048]{1,0:T(8,128)(2,1)} %param.27) | copy-start | bytes 786436
  127.3 89.0 %copy-start.2 = (bf16[2,64,2048]{2,1,0:T(8,128)(2,1)S(1)}, bf16[2,64,2048]{2,1,0:T(8,128)(2,1)}, u32[]{:S(2)}) copy-start(bf16[2,64,2048]{2,1,0:T(8,128)(2,1)} %param.24) | copy-start | bytes 1572868
  164.3 106.7 %all-gather.5.cloned.1.call-start = ((), (), s32[]{:S(2)}) async-start(), calls=%async_computation.8 | async-start | bytes 5013504 | tf_op jit(solution)/shard_map/all_gather | solution.py:58
  166.2 55.9 %copy-start.8 = (bf16[2,64,2048]{2,1,0:T(8,128)(2,1)S(1)}, bf16[2,64,2048]{2,1,0:T(8,128)(2,1)}, u32[]{:S(2)}) copy-start(bf16[2,64,2048]{2,1,0:T(8,128)(2,1)} %param.25) | copy-start | bytes 1572868
  216.3 5.9 %copy-start.1 = (bf16[16,32,2,2,2048]{4,1,3,0,2:T(8,128)(2,1)S(1)}, bf16[16,32,2,2,2048]{4,1,3,0,2:T(8,128)(2,1)}, u32[]{:S(2)}) copy-start(bf16[16,32,2,2,2048]{4,1,3,0,2:T(8,128)(2,1)} %all-gather.3.cloned.1.call-done) | copy-start | bytes 25165828
  289.5 32.5 %copy-start.5 = (bf16[16,128,16]{1,2,0:T(8,128)(2,1)S(1)}, bf16[16,128,16]{1,2,0:T(8,128)(2,1)}, u32[]{:S(2)}) copy-start(bf16[16,128,16]{1,2,0:T(8,128)(2,1)} %get-tuple-element.5) | copy-start | bytes 196612
  289.5 32.8 %copy-start.3 = (bf16[1024,128]{1,0:T(8,128)(2,1)S(1)}, bf16[1024,128]{1,0:T(8,128)(2,1)}, u32[]{:S(2)}) copy-start(bf16[1024,128]{1,0:T(8,128)(2,1)} %param.29) | copy-start | bytes 786436
Sparse Core Ops, SparseCore 0:
  164.4 51.7 all-gather.2
  226.2 44.7 all-gather.4
